TPU v7x, 512 devices: a whole 4x8x8 slice. The times are simulated.
512 devices in a mesh: sp: 32 (over z, x), tp: 16 (over y, core).
Axes of the slice: x: 4, y: 8, z: 8, core: 2. Of those that a mesh axis runs over, the one named last changes fastest.
Arguments:
- glu_value: bfloat16 [1024, 8192], P('tp', 'sp')
- glu_gate: bfloat16 [1024, 8192], P('tp', 'sp'), may hold values from -8 to 8
- conv_taps: float32 [1024, 31], P('tp'), may hold values from -1 to 1
- norm_gain: float32 [1024], P('tp'), may hold values from 0.1 to 1.9
- out_proj: bfloat16 [1024, 2048], P(None, 'tp'), may hold values from -0.1875 to 0.1875
- resid: bfloat16 [8192, 2048], P('sp', 'tp'), may hold values from -6 to 6
- expert_ids: int32 [8192, 2], P('sp'), may hold values from 0 to 31, all different within a row; in each aligned block of 256 rows (0 to 255, 256 to 511, ...) at most 32 rows name the same one
- route_logits: float32 [8192, 2], P('sp'), may hold values from -8 to 8
- group_prob: float32 [8192], P('sp'), may hold values from 0.2 to 1
- w_gate: bfloat16 [32, 2048, 4096], P('sp', None, 'tp'), may hold values from -0.125 to 0.125
- w_up: bfloat16 [32, 2048, 4096], P('sp', None, 'tp'), may hold values from -0.125 to 0.125
- w_down: bfloat16 [32, 4096, 2048], P('sp', None, 'tp'), may hold values from -0.09375 to 0.09375
Outputs:
- layer_out: bfloat16 [8192, 2048], P('sp', 'tp')
Inputs may be any that keep to these rules, and one draw needn't show every extreme that they name: `expert_ids`: each row names 2 different experts. In each aligned block of 256 rows (the rows of one index of sp) no expert is named by more than 32 rows, a bound that some block reaches.
All inputs are finite; a program needn't handle non-finite values.
Results may differ from a plain program's by a relative error of at most 0.0061.
Values may be sent and summed in bfloat16 or wider, within the bound.
A program may use at most 64 MiB of HBM per device.

v0:
```python
import jax
import jax.numpy as jnp
from jax import lax
from jax.sharding import PartitionSpec as P


def from_behind(block, axis, distance):
    devices = range(lax.axis_size(axis))
    route = [(i - distance, i) for i in devices if i - distance in devices]
    return lax.ppermute(block, axis, route)


def from_everyone(shard, axis):
    copies = jnp.broadcast_to(shard, (lax.axis_size(axis), *shard.shape))
    return lax.all_to_all(copies, axis, split_axis=0, concat_axis=0, tiled=True)


def of_everyone(shard, axis):
    everything = from_everyone(shard, axis)
    return jnp.sum(everything, axis=0)


def packed_total(arrays, axis):
    ends = [0]
    for a in arrays:
        ends.append(ends[-1] + a.size)
    subtotal = of_everyone(jnp.concatenate([a.ravel() for a in arrays]), axis)
    return tuple((subtotal[b:e].reshape(a.shape) for a, b, e in zip(arrays, ends, ends[1:])))


def per_device(
    glu_value,
    glu_gate,
    conv_taps,
    norm_gain,
    out_proj,
    resid,
    expert_ids,
    route_logits,
    group_prob,
    w_gate,
    w_up,
    w_down,
):
    local_tokens = glu_value.shape[1]
    tap_count = conv_taps.shape[1]
    channels = glu_value.shape[0] * lax.axis_size("tp")
    gated = (glu_value.astype(jnp.float32) * jax.nn.sigmoid(glu_gate.astype(jnp.float32))).astype(
        jnp.bfloat16
    )
    history = from_behind(gated[:, local_tokens - (tap_count - 1) :], "sp", 1)
    padded = jnp.concatenate([history, gated], axis=1).astype(jnp.float32)
    filtered = jnp.zeros(gated.shape, jnp.float32)
    for offset in range(tap_count):
        filtered = (
            filtered + conv_taps[:, offset : offset + 1] * padded[:, offset : offset + local_tokens]
        )
    total_one, total_two = packed_total(
        (jnp.sum(filtered, axis=0), jnp.sum(filtered * filtered, axis=0)), "tp"
    )
    mean = total_one / channels
    var = total_two / channels - mean * mean
    normed = (filtered - mean[None, :]) * lax.rsqrt(var[None, :] + 1e-05) * norm_gain[:, None]
    activated = jax.nn.silu(normed).astype(jnp.bfloat16)
    weights = out_proj
    projected = lax.dot_general(
        lax.all_gather(activated, "tp", axis=0, tiled=True),
        weights,
        (((0,), (0,)), ((), ())),
        preferred_element_type=jnp.float32,
    )
    mixed = (resid.astype(jnp.float32) + projected).astype(jnp.bfloat16)
    experts = lax.axis_size("sp")
    capacity = 4 * local_tokens // experts
    flat_ids = expert_ids.reshape(-1)
    onehot = (flat_ids[:, None] == jnp.arange(experts, dtype=jnp.int32)[None, :]).astype(jnp.int32)
    rank = jnp.sum(jnp.cumsum(onehot, axis=0) * onehot, axis=1) - 1
    slot = flat_ids * capacity + rank
    token_of = jnp.arange(flat_ids.shape[0], dtype=jnp.int32) // expert_ids.shape[1]
    table = jnp.zeros((experts * capacity,), jnp.int32).at[slot].set(token_of)
    filled = jnp.zeros((experts * capacity,), jnp.bool_).at[slot].set(True)
    route_weight = (group_prob[:, None] * jax.nn.softmax(route_logits, axis=-1)).reshape(-1)
    outgoing = jnp.where(
        filled[:, None], jnp.take(mixed, table, axis=0), jnp.zeros((), jnp.bfloat16)
    )
    outgoing = outgoing.reshape(experts, capacity, mixed.shape[1])
    rows = lax.all_gather(
        lax.all_to_all(outgoing, "sp", split_axis=0, concat_axis=0, tiled=True),
        "tp",
        axis=2,
        tiled=True,
    )
    sources, count, width = rows.shape
    flat_rows = rows.reshape(sources * count, width)
    gate_part = jnp.dot(flat_rows, w_gate[0], preferred_element_type=jnp.float32)
    up_part = jnp.dot(flat_rows, w_up[0], preferred_element_type=jnp.float32)
    hidden = (jax.nn.silu(gate_part) * up_part).astype(jnp.bfloat16)
    weights = w_down[0]
    expert_out = jnp.dot(
        lax.all_gather(hidden, "tp", axis=1, tiled=True),
        weights,
        preferred_element_type=jnp.float32,
    )
    results = expert_out.astype(jnp.bfloat16).reshape(sources, count, w_down.shape[2])
    returned = lax.all_to_all(results, "sp", split_axis=0, concat_axis=0, tiled=True)
    flat_back = returned.reshape(experts * capacity, returned.shape[2])
    picked = jnp.take(flat_back, slot, axis=0).astype(jnp.float32) * route_weight[:, None]
    routed = jnp.sum(picked.reshape(local_tokens, expert_ids.shape[1], flat_back.shape[1]), axis=1)
    return (mixed.astype(jnp.float32) + routed).astype(jnp.bfloat16)


def solution(mesh):
    return jax.shard_map(
        per_device,
        mesh=mesh,
        in_specs=(
            P("tp", "sp"),
            P("tp", "sp"),
            P("tp", None),
            P("tp"),
            P(None, "tp"),
            P("sp", "tp"),
            P("sp", None),
            P("sp", None),
            P("sp"),
            P("sp", None, "tp"),
            P("sp", None, "tp"),
            P("sp", None, "tp"),
        ),
        out_specs=P("sp", "tp"),
        check_vma=False,
    )
```

profile of v0, /device:TPU:1, one launch (start us, length us, event | category | flops | bytes accessed | tf_op | source)
XLA Modules:
  0.0 237.7 jit_solution(12596920624349899466)
XLA Ops:
  6.5 0.9 multiply_convert_fusion.1
  7.5 0.1 slice.272
  7.5 3.9 %collective-permute-start = (bf16[64,30]{1,0:T(8,128)(2,1)S(1)}, bf16[64,30]{1,0:T(8,128)(2,1)S(1)}, u32[]{:S(2)}, u32[]{:S(2)}) collective-permute-start(bf16[64,30]{1,0:T(8,128)(2,1)S(1)} %slice.272), channel_id=1, source_target_pairs={{0,16},{16,32},{32,48},{48,64},{64,80},{80,96},{96,112},{112,128},... | collective-permute-start | bytes 11528 | tf_op jit(solution)/shard_map/ppermute | solution.py:10
  11.5 1.0 slice_bitcast_fusion.30
  12.5 1.0 slice_bitcast_fusion.29
  13.4 0.8 copy.32
  14.3 0.1 eq.26
  14.4 0.1 reshape.114
  14.5 0.7 broadcast_multiply_fusion
  15.2 1.2 reduce-window.6
  16.4 0.2 slice_reduce_fusion
  16.7 0.1 fusion.7
  16.8 0.1 copy.37
  16.9 0.1 mul.489
  17.1 2.4 %scatter_custom_fusion.1 = s32[1024]{0:T(1024)S(1)} fusion(s32[512]{0:T(512)S(1)} %bitcast.102, s32[512]{0:T(512)S(1)} %add_select_fusion, s32[]{:T(128)} %constant.68.clone.1), kind=kCustom, calls=%fused_computation.106 | custom fusion | bytes 4100 | tf_op jit(solution)/shard_map/scatter | solution.py:80
  19.6 0.1 maximum_convert_fusion
  19.7 0.9 fusion.48
  20.6 0.6 broadcast_in_dim.60
  21.2 8.1 %all-to-all-start = ((f32[16,1,512]{2,1,0:T(1,128)}), f32[16,1,512]{2,1,0:T(1,128)S(1)}, u32[]{:S(2)}, u32[]{:S(2)}) async-start(f32[16,1,512]{2,1,0:T(1,128)} %broadcast_in_dim.60), calls=%async_computation | async-start | bytes 65536 | tf_op jit(solution)/shard_map/all_to_all | solution.py:15
  29.3 0.0 all-gather.3.cloned.1.call-start
  29.3 0.1 broadcast_in_dim.67
  29.4 2.4 %scatter_custom_fusion = pred[1024]{0:T(1024)(128)(4,1)S(1)} fusion(s32[512]{0:T(512)S(1)} %bitcast.103, pred[512]{0:T(512)(128)(4,1)S(1)} %broadcast.121, pred[]{:T(512)} %constant.72.clone.1), kind=kCustom, calls=%fused_computation.109 | custom fusion | bytes 1025 | tf_op jit(solution)/shard_map/scatter | solution.py:81
  31.9 0.1 broadcast_in_dim.64
  31.9 4.7 %all-to-all-done = f32[16,1,512]{2,1,0:T(1,128)S(1)} async-done(((f32[16,1,512]{2,1,0:T(1,128)}), f32[16,1,512]{2,1,0:T(1,128)S(1)}, u32[]{:S(2)}, u32[]{:S(2)}) %all-to-all-start) | async-done | bytes 32800 | tf_op jit(solution)/shard_map/all_to_all | solution.py:15
  36.7 0.8 multiply_convert_fusion
  37.5 16.3 %all_gather.9 = bf16[1024,256]{1,0:T(8,128)(2,1)S(1)} all-gather(bf16[64,256]{1,0:T(8,128)(2,1)S(1)} %multiply_convert_fusion), channel_id=1, replica_groups=mesh['sp'=32,'tp'=16] {'tp'}, dimensions={0}, use_global_device_ids=true | all-gather | bytes 557056 | tf_op jit(solution)/shard_map/all_gather | solution.py:67
  53.8 0.3 fusion.1
  54.1 3.2 %gather_fusion = bf16[1024,128]{1,0:T(8,128)(2,1)S(1)} fusion(bf16[256,128]{1,0:T(8,128)(2,1)S(1)} %fusion.1, s32[1024]{0:T(1024)S(1)} %fusion.39), kind=kCustom, calls=%fused_computation | custom fusion | bytes 528384 | tf_op jit(solution)/shard_map/jit(_take)/gather | solution.py:84
  57.4 0.3 select_select_fusion
  57.7 0.0 copy-start.7
  57.7 24.3 %all_to_all.16 = bf16[32,32,128]{2,1,0:T(8,128)(2,1)} all-to-all(bf16[32,32,128]{2,1,0:T(8,128)(2,1)S(1)} %select_select_fusion), channel_id=1, replica_groups=mesh['sp'=32,'tp'=16] {'sp'}, dimensions={0} | all-to-all | bytes 524288 | tf_op jit(solution)/shard_map/all_to_all | solution.py:88
  82.0 0.0 all-gather.3.cloned.1.call-update
  82.0 0.0 all-gather.5.cloned.1.call-start
  82.1 46.9 %all-gather.3.cloned.1.call-done = bf16[32,32,2048]{2,1,0:T(8,128)(2,1)} async-done(((bf16[32,32,128]{2,1,0:T(8,128)(2,1)}), bf16[32,32,2048]{2,1,0:T(8,128)(2,1)}) %all-gather.3.cloned.1.call-update) | async-done | bytes 4194320 | tf_op jit(solution)/shard_map/all_gather | solution.py:87
  129.0 3.6 %fusion.4 = f32[1024,256]{1,0:T(8,128)S(1)} fusion(bf16[1024,2048]{1,0:T(8,128)(2,1)} %bitcast.105, bf16[1,2048,256]{2,1,0:T(8,128)(2,1)S(1)} %copy-done), kind=kOutput, calls=%fused_computation.11 | convolution fusion | flops 1073741824 | bytes 6291456 | tf_op jit(solution)/shard_map/dot_general | solution.py:95
  132.6 2.1 fusion
  134.7 0.0 all-gather.5.cloned.1.call-update
  134.8 0.1 sub.37
  134.9 0.1 copy.35
  135.0 67.3 %all-gather.5.cloned.1.call-done = bf16[1024,4096]{1,0:T(8,128)(2,1)} async-done(((bf16[1024,256]{1,0:T(8,128)(2,1)}), bf16[1024,4096]{1,0:T(8,128)(2,1)}) %all-gather.5.cloned.1.call-update) | async-done | bytes 8388624 | tf_op jit(solution)/shard_map/all_gather | solution.py:100
  202.3 6.6 %convolution_convert_fusion = bf16[1024,128]{1,0:T(8,128)(2,1)} fusion(bf16[1024,4096]{1,0:T(8,128)(2,1)} %all-gather.5.cloned.1.call-done, bf16[1,4096,128]{2,1,0:T(8,128)(2,1)} %param.23), kind=kOutput, calls=%fused_computation.6 | convolution fusion | flops 1073872896 | bytes 9699328 | tf_op jit(solution)/shard_map/dot_general | solution.py:99
  208.9 6.8 %all-to-all-start.2 = ((bf16[32,32,128]{2,1,0:T(8,128)(2,1)}), bf16[32,32,128]{2,1,0:T(8,128)(2,1)S(1)}, u32[]{:S(2)}, u32[]{:S(2)}) async-start(bf16[32,32,128]{2,1,0:T(8,128)(2,1)} %bitcast.39), calls=%async_computation.2 | async-start | bytes 524288 | tf_op jit(solution)/shard_map/all_to_all | solution.py:105
  215.8 0.2 copy.36
  216.1 0.1 copy.38
  216.2 11.2 %all-to-all-done.2 = bf16[32,32,128]{2,1,0:T(8,128)(2,1)S(1)} async-done(((bf16[32,32,128]{2,1,0:T(8,128)(2,1)}), bf16[32,32,128]{2,1,0:T(8,128)(2,1)S(1)}, u32[]{:S(2)}, u32[]{:S(2)}) %all-to-all-start.2) | async-done | bytes 262176 | tf_op jit(solution)/shard_map/all_to_all | solution.py:105
  227.4 1.3 gather_fusion.1
  228.8 1.5 multiply_reduce_fusion
  230.2 0.7 add_convert_fusion
  (33 shorter events, 0.3 us)
Async XLA Ops:
  6.5 122.4 %copy-start = (bf16[1,2048,256]{2,1,0:T(8,128)(2,1)S(1)}, bf16[1,2048,256]{2,1,0:T(8,128)(2,1)}, u32[]{:S(2)}) copy-start(bf16[1,2048,256]{2,1,0:T(8,128)(2,1)} %param.21) | copy-start | bytes 3145732
  6.5 47.2 %copy-start.1 = (bf16[1024,128]{1,0:T(8,128)(2,1)S(1)}, bf16[1024,128]{1,0:T(8,128)(2,1)}, u32[]{:S(2)}) copy-start(bf16[1024,128]{1,0:T(8,128)(2,1)} %param.16) | copy-start | bytes 786436
  6.5 47.2 %copy-start.2 = (bf16[256,128]{1,0:T(8,128)(2,1)S(1)}, bf16[256,128]{1,0:T(8,128)(2,1)}, u32[]{:S(2)}) copy-start(bf16[256,128]{1,0:T(8,128)(2,1)} %param.17) | copy-start | bytes 196612
  7.5 12.0 %collective-permute-start = (bf16[64,30]{1,0:T(8,128)(2,1)S(1)}, bf16[64,30]{1,0:T(8,128)(2,1)S(1)}, u32[]{:S(2)}, u32[]{:S(2)}) collective-permute-start(bf16[64,30]{1,0:T(8,128)(2,1)S(1)} %slice.272), channel_id=1, source_target_pairs={{0,16},{16,32},{32,48},{48,64},{64,80},{80,96},{96,112},{112,128},... | collective-permute-start | bytes 11528 | tf_op jit(solution)/shard_map/ppermute | solution.py:10
  21.2 15.5 %all-to-all-start = ((f32[16,1,512]{2,1,0:T(1,128)}), f32[16,1,512]{2,1,0:T(1,128)S(1)}, u32[]{:S(2)}, u32[]{:S(2)}) async-start(f32[16,1,512]{2,1,0:T(1,128)} %broadcast_in_dim.60), calls=%async_computation | async-start | bytes 65536 | tf_op jit(solution)/shard_map/all_to_all | solution.py:15
  29.3 99.7 %all-gather.3.cloned.1.call-start = ((), (), s32[]{:S(2)}) async-start(), calls=%async_computation.3 | async-start | bytes 4456448 | tf_op jit(solution)/shard_map/all_gather | solution.py:87
  57.7 74.9 %copy-start.7 = (bf16[1,2048,256]{2,1,0:T(8,128)(2,1)S(1)}, bf16[1,2048,256]{2,1,0:T(8,128)(2,1)}, u32[]{:S(2)}) copy-start(bf16[1,2048,256]{2,1,0:T(8,128)(2,1)} %param.22) | copy-start | bytes 3145732
  82.0 120.3 %all-gather.5.cloned.1.call-start = ((), (), s32[]{:S(2)}) async-start(), calls=%async_computation.4 | async-start | bytes 8912896 | tf_op jit(solution)/shard_map/all_gather | solution.py:100
  129.0 3.6 %copy-start.6 = (bf16[32,32,2048]{2,1,0:T(8,128)(2,1)S(1)}, bf16[32,32,2048]{2,1,0:T(8,128)(2,1)}, u32[]{:S(2)}) copy-start(bf16[32,32,2048]{2,1,0:T(8,128)(2,1)} %all-gather.3.cloned.1.call-done) | copy-start | bytes 12582916
  135.0 80.8 %copy-start.3 = (s32[256,2]{0,1:T(2,128)S(1)}, s32[256,2]{0,1:T(2,128)}, u32[]{:S(2)}) copy-start(s32[256,2]{0,1:T(2,128)} %param.18) | copy-start | bytes 6148
  135.0 81.0 %copy-start.4 = (f32[256,2]{0,1:T(2,128)S(1)}, f32[256,2]{0,1:T(2,128)}, u32[]{:S(2)}) copy-start(f32[256,2]{0,1:T(2,128)} %param.19) | copy-start | bytes 6148
  135.0 81.1 %copy-start.5 = (f32[256]{0:T(256)S(1)}, f32[256]{0:T(256)}, u32[]{:S(2)}) copy-start(f32[256]{0:T(256)} %param.20) | copy-start | bytes 3076
  208.9 18.5 %all-to-all-start.2 = ((bf16[32,32,128]{2,1,0:T(8,128)(2,1)}), bf16[32,32,128]{2,1,0:T(8,128)(2,1)S(1)}, u32[]{:S(2)}, u32[]{:S(2)}) async-start(bf16[32,32,128]{2,1,0:T(8,128)(2,1)} %bitcast.39), calls=%async_computation.2 | async-start | bytes 524288 | tf_op jit(solution)/shard_map/all_to_all | solution.py:105
Sparse Core Ops, SparseCore 0:
  82.1 46.7 all-gather.2
  134.9 67.3 all-gather.4
where the time goes:
time: 239 us; the launch traced here: 238 us
  waiting for transfers between devices  130 us (54%)
  blocking collectives  40.6 us (17%)
  starting transfers between devices  18.9 us (8%)
  local copies, waits for them, and re-layouts  14.4 us (6%)
  between operations  13.7 us (6%)
  matrix products  12.7 us (5%)
  other arithmetic  7.23 us (3%)
    all_gather x1, waiting for transfers between devices, per_device(): lax.all_gather(hidden, 'tp', axis=1, tiled=True)  67.3 us
    all_gather x1, waiting for transfers between devices, per_device(): lax.all_gather(lax.all_to_all(outgoing, 'sp', split_axis=0, concat_axis=0...  46.9 us
    all_to_all x1, blocking collectives, per_device(): lax.all_to_all(outgoing, 'sp', split_axis=0, concat_axis=0, tiled=True)  24.3 us
    all_gather x1, blocking collectives, per_device(): lax.all_gather(activated, 'tp', axis=0, tiled=True)  16.3 us
    all_to_all x1, waiting for transfers between devices, per_device(): lax.all_to_all(results, 'sp', split_axis=0, concat_axis=0, tiled=True)  11.2 us
    all_to_all x1, starting transfers between devices, from_everyone(): return lax.all_to_all(copies, axis, split_axis=0, concat_axis=0, tiled=True)  8.07 us
    all_to_all x1, starting transfers between devices, per_device(): lax.all_to_all(results, 'sp', split_axis=0, concat_axis=0, tiled=True)  6.83 us
    dot_general x1, matrix products, per_device(): jnp.dot(lax.all_gather(hidden, 'tp', axis=1, tiled=True), weights, prefer...  6.65 us
  transfers between devices with their start and end apart: 5, of which 4 were waited for; matrix products, arithmetic and copies ran while one was open for 5% of the time, Pallas kernels for 0%

commit v1 on v0

v1 whole, which is shorter than its diff:
```python
import functools
import jax
import jax.numpy as jnp
from jax import lax
from jax.experimental import pallas as pl
from jax.experimental.pallas import tpu as pltpu
from jax.sharding import PartitionSpec as P

BF = jnp.bfloat16
F32 = jnp.float32
MESH = pl.DeviceIdType.MESH


def from_behind(block, axis, distance):
    devices = range(lax.axis_size(axis))
    route = [(i - distance, i) for i in devices if i - distance in devices]
    return lax.ppermute(block, axis, route)


def from_everyone(shard, axis):
    copies = jnp.broadcast_to(shard, (lax.axis_size(axis), *shard.shape))
    return lax.all_to_all(copies, axis, split_axis=0, concat_axis=0, tiled=True)


def of_everyone(shard, axis):
    everything = from_everyone(shard, axis)
    return jnp.sum(everything, axis=0)


def packed_total(arrays, axis):
    ends = [0]
    for a in arrays:
        ends.append(ends[-1] + a.size)
    subtotal = of_everyone(jnp.concatenate([a.ravel() for a in arrays]), axis)
    return tuple((subtotal[b:e].reshape(a.shape) for a, b, e in zip(arrays, ends, ends[1:])))


def dot(a, b):
    return jnp.dot(a, b, preferred_element_type=F32)


def moe_kernel(
    dims,
    mixed_ref,
    ids_ref,
    idst_ref,
    logits_ref,
    prob_ref,
    wg_hbm,
    wu_hbm,
    wd_hbm,
    out_ref,
    wg,
    wu,
    wd,
    outg,
    rows,
    hid,
    res,
    ret,
    wsem,
    dsend,
    drecv,
    rring,
    rsib,
    rsend,
    hring,
    hsib,
    hsend,
    bsend,
    brecv,
):
    nx, nz, ny, cap = dims
    experts = nx * nz
    chunk = nx * cap
    ha = ny // 2
    hb = ny - 1 - ha
    tokens, width = mixed_ref.shape
    ffw = wg.shape[1]
    s = lax.axis_index("sp")
    j = lax.axis_index("tp")
    z, x = s // nx, s % nx
    y, c = j // 2, j % 2
    sib = 2 * y + (1 - c)

    barrier = pltpu.get_barrier_semaphore()

    def greet(k, carry):
        pl.semaphore_signal(barrier, inc=1, device_id=((s + k) % experts, j), device_id_type=MESH)
        return carry

    lax.fori_loop(1, experts, greet, 0)
    for tgt in (2 * ((y + 1) % ny) + c, 2 * ((y + ny - 1) % ny) + c, sib):
        pl.semaphore_signal(barrier, inc=1, device_id=(s, tgt), device_id_type=MESH)

    loads = [
        pltpu.make_async_copy(a.at[0], b, wsem.at[n])
        for n, (a, b) in enumerate(((wg_hbm, wg), (wu_hbm, wu), (wd_hbm, wd)))
    ]
    for load in loads:
        load.start()

    def offset(i):
        return ((i + 1) // 2) * (1 - 2 * ((i + 1) % 2))

    id0 = idst_ref[0:1, :]
    id1 = idst_ref[1:2, :]
    e_io = lax.broadcasted_iota(jnp.int32, (experts, tokens), 0)
    named = jnp.where((e_io == id0) | (e_io == id1), 1.0, 0.0)
    r_io = lax.broadcasted_iota(jnp.int32, (tokens, tokens), 0)
    c_io = lax.broadcasted_iota(jnp.int32, (tokens, tokens), 1)
    upper = jnp.where(r_io < c_io, 1.0, 0.0).astype(BF)
    before = dot(named.astype(BF), upper)
    slot0 = jnp.sum(jnp.where(e_io == id0, before, 0.0), axis=0, keepdims=True) + id0.astype(F32) * cap
    slot1 = jnp.sum(jnp.where(e_io == id1, before, 0.0), axis=0, keepdims=True) + id1.astype(F32) * cap
    s_io = lax.broadcasted_iota(jnp.int32, (experts * cap, tokens), 0).astype(F32)
    pick = jnp.where((s_io == slot0) | (s_io == slot1), 1.0, 0.0).astype(BF)
    outg[...] = dot(pick, mixed_ref[...]).astype(BF)
    own_col = pl.ds(pl.multiple_of(j * width, width), width)
    own_row = pl.ds(pl.multiple_of(x * cap, cap), cap)
    rows[z, own_row, own_col] = outg[pl.ds(pl.multiple_of(s * cap, cap), cap), :]

    pl.semaphore_wait(barrier, experts - 1 + 3)

    def dispatch(n, carry):
        i, dx = n // nx, n % nx
        zt = (z - offset(i) + nz) % nz
        xt = (x + dx) % nx
        e = zt * nx + xt
        pltpu.make_async_remote_copy(
            src_ref=outg.at[pl.ds(pl.multiple_of(e * cap, cap), cap), :],
            dst_ref=rows.at[z, own_row, own_col],
            send_sem=dsend,
            recv_sem=drecv.at[z],
            device_id=(e, j),
            device_id_type=MESH,
        ).start()
        return carry

    lax.fori_loop(1, experts, dispatch, 0)

    def block(buf, wide, q, origin):
        return buf.at[q, :, pl.ds(pl.multiple_of(origin * wide, wide), wide)]

    def push(buf, wide, q, i, origin_y, hop, leg, ring, send, sgn):
        ref = block(buf, wide, q, 2 * origin_y + c)
        step = sgn * (1 - 2 * leg)
        pltpu.make_async_remote_copy(
            src_ref=ref,
            dst_ref=ref,
            send_sem=send.at[i],
            recv_sem=ring.at[i, leg * ha + hop],
            device_id=(s, 2 * ((y + step + ny) % ny) + c),
            device_id_type=MESH,
        ).start()

    def share(buf, wide, q, i, origin_y, sem, send):
        ref = block(buf, wide, q, 2 * origin_y + c)
        pltpu.make_async_remote_copy(
            src_ref=ref,
            dst_ref=ref,
            send_sem=send.at[i],
            recv_sem=sem.at[i],
            device_id=(s, sib),
            device_id_type=MESH,
        ).start()

    def arrived(ref, sem):
        pltpu.make_async_copy(ref, ref, sem).wait()

    def open_ring(buf, wide, q, i, ring, sibs, send):
        sgn = 1 - 2 * (i % 2)
        push(buf, wide, q, i, y, 0, 0, ring, send, sgn)
        if hb > 0:
            push(buf, wide, q, i, y, 0, 1, ring, send, sgn)
        share(buf, wide, q, i, y, sibs, send)

    def hop_ring(h, buf, wide, q, i, ring, sibs, send):
        sgn = 1 - 2 * (i % 2)
        for leg, reach in ((0, ha), (1, hb)):
            if h > reach:
                continue
            origin = (y - sgn * (1 - 2 * leg) * h + 2 * ny) % ny
            arrived(block(buf, wide, q, 2 * origin + c), ring.at[i, leg * ha + h - 1])
            if h < reach:
                push(buf, wide, q, i, origin, h, leg, ring, send, sgn)
            share(buf, wide, q, i, origin, sibs, send)

    def tick(t, carry):
        def at(stage, body):
            i = t - stage

            @pl.when((i >= 0) & (i < nz))
            def _():
                body(i, (z + offset(i) + nz) % nz)

        def rows_open(i, q):
            @pl.when(i == 0)
            def _():
                if nx > 1:
                    arrived(outg.at[pl.ds(0, (nx - 1) * cap), :], drecv.at[q])

            @pl.when(i > 0)
            def _():
                arrived(outg.at[pl.ds(0, nx * cap), :], drecv.at[q])

            open_ring(rows, width, q, i, rring, rsib, rsend)

        def rows_hop(h, i, q):
            hop_ring(h, rows, width, q, i, rring, rsib, rsend)

        def hid_hop(h, i, q):
            hop_ring(h, hid, ffw, q, i, hring, hsib, hsend)

        def first(i, q):
            @pl.when(i == 0)
            def _():
                loads[0].wait()
                loads[1].wait()

            arrived(rows.at[q, :, pl.ds(0, ny * width)], rsib.at[i])
            r = rows[q]
            g = dot(r, wg[...])
            u = dot(r, wu[...])
            h = (g / (1.0 + jnp.exp(-g))) * u
            hid[q, :, pl.ds(pl.multiple_of(j * ffw, ffw), ffw)] = h.astype(BF)
            open_ring(hid, ffw, q, i, hring, hsib, hsend)

        def second(i, q):
            @pl.when(i == 0)
            def _():
                loads[2].wait()

            arrived(hid.at[q, :, pl.ds(0, ny * ffw)], hsib.at[i])
            res[i] = dot(hid[q], wd[...]).astype(BF)
            for xt in range(nx):
                tgt = q * nx + xt
                dst = ret.at[pl.ds(pl.multiple_of(s * cap, cap), cap), :]

                @pl.when(tgt == s)
                def _():
                    ret[pl.ds(pl.multiple_of(s * cap, cap), cap), :] = res[i, pl.ds(xt * cap, cap), :]

                @pl.when(tgt != s)
                def _():
                    pltpu.make_async_remote_copy(
                        src_ref=res.at[i, pl.ds(xt * cap, cap), :],
                        dst_ref=dst,
                        send_sem=bsend,
                        recv_sem=brecv,
                        device_id=(tgt, j),
                        device_id_type=MESH,
                    ).start()

        at(0, rows_open)
        for h in range(1, ha + 1):
            at(h, functools.partial(rows_hop, h))
        for h in range(1, ha + 1):
            at(ha + 1 + h, functools.partial(hid_hop, h))
        at(2 * ha + 2, second)
        at(ha + 1, first)
        return carry

    lax.fori_loop(0, nz + 2 * ha + 2, tick, 0)

    id0 = ids_ref[:, 0:1]
    id1 = ids_ref[:, 1:2]
    e_io = lax.broadcasted_iota(jnp.int32, (tokens, experts), 1)
    named = jnp.where((e_io == id0) | (e_io == id1), 1.0, 0.0)
    lower = jnp.where(c_io < r_io, 1.0, 0.0).astype(BF)
    before = dot(lower, named.astype(BF))
    slot0 = jnp.sum(jnp.where(e_io == id0, before, 0.0), axis=1, keepdims=True) + id0.astype(F32) * cap
    slot1 = jnp.sum(jnp.where(e_io == id1, before, 0.0), axis=1, keepdims=True) + id1.astype(F32) * cap
    s_io = lax.broadcasted_iota(jnp.int32, (tokens, experts * cap), 1).astype(F32)
    pick0 = jnp.where(s_io == slot0, 1.0, 0.0).astype(BF)
    pick1 = jnp.where(s_io == slot1, 1.0, 0.0).astype(BF)
    l0 = logits_ref[:, 0:1]
    l1 = logits_ref[:, 1:2]
    top = jnp.maximum(l0, l1)
    e0 = jnp.exp(l0 - top)
    e1 = jnp.exp(l1 - top)
    scale = prob_ref[...] / (e0 + e1)
    far = outg.at[pl.ds(0, (experts - 1) * cap), :]
    arrived(far, brecv)
    back = ret[...]
    routed = dot(pick0, back) * (e0 * scale) + dot(pick1, back) * (e1 * scale)
    out_ref[...] = (mixed_ref[...].astype(F32) + routed).astype(BF)

    arrived(far, dsend)
    arrived(far, bsend)

    def drain(i, carry):
        arrived(rows.at[0, :, pl.ds(0, (2 * ny - 1) * width)], rsend.at[i])
        arrived(hid.at[0, :, pl.ds(0, (2 * ny - 1) * ffw)], hsend.at[i])
        return carry

    lax.fori_loop(0, nz, drain, 0)


def moe(mixed, ids, logits, prob, w_gate, w_up, w_down):
    sp, tp = lax.axis_size("sp"), lax.axis_size("tp")
    nx = 4 if sp % 8 == 0 else 1
    nz, ny = sp // nx, tp // 2
    tokens, width = mixed.shape
    cap = 4 * tokens // sp
    depth, ffw = w_gate.shape[1:]
    chunk = nx * cap
    ha = ny // 2
    dma = pltpu.SemaphoreType.DMA
    vmem = pl.BlockSpec(memory_space=pltpu.VMEM)
    hbm = pl.BlockSpec(memory_space=pl.ANY)
    return pl.pallas_call(
        functools.partial(moe_kernel, (nx, nz, ny, cap)),
        out_shape=jax.ShapeDtypeStruct((tokens, width), BF),
        in_specs=[vmem] * 5 + [hbm] * 3,
        out_specs=vmem,
        scratch_shapes=[
            pltpu.VMEM((depth, ffw), BF),
            pltpu.VMEM((depth, ffw), BF),
            pltpu.VMEM(w_down.shape[1:], BF),
            pltpu.VMEM((sp * cap, width), BF),
            pltpu.VMEM((nz, chunk, depth), BF),
            pltpu.VMEM((nz, chunk, tp * ffw), BF),
            pltpu.VMEM((nz, chunk, width), BF),
            pltpu.VMEM((sp * cap, width), BF),
            dma((3,)),
            dma(()),
            dma((nz,)),
            dma((nz, ny - 1)),
            dma((nz,)),
            dma((nz,)),
            dma((nz, ny - 1)),
            dma((nz,)),
            dma((nz,)),
            dma(()),
            dma(()),
        ],
        compiler_params=pltpu.CompilerParams(
            collective_id=0, has_side_effects=True, vmem_limit_bytes=40 * 1024 * 1024
        ),
    )(mixed, ids, ids.T, logits, prob[:, None], w_gate, w_up, w_down)


def per_device(
    glu_value,
    glu_gate,
    conv_taps,
    norm_gain,
    out_proj,
    resid,
    expert_ids,
    route_logits,
    group_prob,
    w_gate,
    w_up,
    w_down,
):
    local_tokens = glu_value.shape[1]
    tap_count = conv_taps.shape[1]
    channels = glu_value.shape[0] * lax.axis_size("tp")
    gated = (glu_value.astype(F32) * jax.nn.sigmoid(glu_gate.astype(F32))).astype(BF)
    history = from_behind(gated[:, local_tokens - (tap_count - 1) :], "sp", 1)
    padded = jnp.concatenate([history, gated], axis=1).astype(F32)
    filtered = jnp.zeros(gated.shape, F32)
    for offset in range(tap_count):
        filtered = (
            filtered + conv_taps[:, offset : offset + 1] * padded[:, offset : offset + local_tokens]
        )
    total_one, total_two = packed_total(
        (jnp.sum(filtered, axis=0), jnp.sum(filtered * filtered, axis=0)), "tp"
    )
    mean = total_one / channels
    var = total_two / channels - mean * mean
    normed = (filtered - mean[None, :]) * lax.rsqrt(var[None, :] + 1e-05) * norm_gain[:, None]
    activated = jax.nn.silu(normed).astype(BF)
    projected = lax.dot_general(
        lax.all_gather(activated, "tp", axis=0, tiled=True),
        out_proj,
        (((0,), (0,)), ((), ())),
        preferred_element_type=F32,
    )
    mixed = (resid.astype(F32) + projected).astype(BF)
    return moe(mixed, expert_ids, route_logits, group_prob, w_gate, w_up, w_down)


def solution(mesh):
    return jax.shard_map(
        per_device,
        mesh=mesh,
        in_specs=(
            P("tp", "sp"),
            P("tp", "sp"),
            P("tp", None),
            P("tp"),
            P(None, "tp"),
            P("sp", "tp"),
            P("sp", None),
            P("sp", None),
            P("sp"),
            P("sp", None, "tp"),
            P("sp", None, "tp"),
            P("sp", None, "tp"),
        ),
        out_specs=P("sp", "tp"),
        check_vma=False,
    )
```

time: 239 us -> 150 us (0.63)
  waiting for transfers between devices: 130 us -> 6.63 us
  Pallas kernels: 0 us -> 103 us
  blocking collectives: 40.6 us -> 16.3 us
  between operations: 13.7 us -> 0.17 us
  matrix products: 12.7 us -> 1.18 us
  local copies, waits for them, and re-layouts: 14.4 us -> 4.92 us
  starting transfers between devices: 18.9 us -> 12.7 us
  other arithmetic: 7.23 us -> 4.21 us
    all_gather x2 -> x0, waiting for transfers between devices: 114 us -> none  [the longest x1 67.3 us: per_device(): lax.all_gather(hidden, 'tp', axis=1, tiled=True)]
    pallas_call x0 -> x1, Pallas kernels: none -> 103 us  [moe(): pl.pallas_call(functools.partial(moe_kernel, (nx, nz, ny, cap)), out_shap...]
    all_to_all x1 -> x0, blocking collectives: 24.3 us -> none  [per_device(): lax.all_to_all(outgoing, 'sp', split_axis=0, concat_axis=0, tiled=True)]
    dot_general x4 -> x1, matrix products: 12.7 us -> 1.18 us  [per_device(): lax.dot_general(lax.all_gather(activated, 'tp', axis=0, tiled=True), out_...]
    all_to_all x1 -> x0, waiting for transfers between devices: 11.2 us -> none  [per_device(): lax.all_to_all(results, 'sp', split_axis=0, concat_axis=0, tiled=True)]
    all_to_all x1 -> x0, starting transfers between devices: 6.83 us -> none  [per_device(): lax.all_to_all(results, 'sp', split_axis=0, concat_axis=0, tiled=True)]
    scatter x2 -> x0, local copies, waits for them, and re-layouts: 4.89 us -> none  [the longest x1 2.45 us: per_device(): filled = jnp.zeros((experts * capacity,), jnp.bool_).at[slot].set(True)]
    gather x2 -> x0, local copies, waits for them, and re-layouts: 4.54 us -> none  [the longest x1 3.21 us: per_device(): jnp.take(mixed, table, axis=0)]
  transfers between devices with their start and end apart: 5 -> 2, of which waited for: 4 -> 2; matrix products, arithmetic and copies ran while one was open for 5% -> 1% of each run, Pallas kernels for 0% -> 0%
where the time goes in v1:
time: 150 us; the launch traced here: 149 us
  Pallas kernels  103 us (69%)
  blocking collectives  16.3 us (11%)
  starting transfers between devices  12.7 us (8%)
  waiting for transfers between devices  6.63 us (4%)
  local copies, waits for them, and re-layouts  4.92 us (3%)
  other arithmetic  4.21 us (3%)
    pallas_call x1, Pallas kernels, moe(): pl.pallas_call(functools.partial(moe_kernel, (nx, nz, ny, cap)), out_shap...  103 us
    all_gather x1, blocking collectives, per_device(): lax.all_gather(activated, 'tp', axis=0, tiled=True)  16.3 us
    all_to_all x1, starting transfers between devices, from_everyone(): return lax.all_to_all(copies, axis, split_axis=0, concat_axis=0, tiled=True)  8.77 us
    all_to_all x1, waiting for transfers between devices, from_everyone(): return lax.all_to_all(copies, axis, split_axis=0, concat_axis=0, tiled=True)  5.83 us
    ppermute x1, starting transfers between devices, from_behind(): return lax.ppermute(block, axis, route)  3.92 us
    unnamed x25, local copies, waits for them, and re-layouts  3.41 us
  transfers between devices with their start and end apart: 2, of which 2 were waited for; matrix products, arithmetic and copies ran while one was open for 1% of the time, Pallas kernels for 0%

profile of v1, /device:TPU:1, one launch (start us, length us, event | category | flops | bytes accessed | tf_op | source)
XLA Modules:
  0.0 149.2 jit_solution(11495929593314915500)
XLA Ops:
  0.0 0.0 copy-start
  0.0 0.8 multiply_convert_fusion.1
  0.9 0.0 copy-start.7
  0.9 0.1 slice.260
  0.9 3.9 %collective-permute-start = (bf16[64,30]{1,0:T(8,128)(2,1)S(1)}, bf16[64,30]{1,0:T(8,128)(2,1)S(1)}, u32[]{:S(2)}, u32[]{:S(2)}) collective-permute-start(bf16[64,30]{1,0:T(8,128)(2,1)S(1)} %slice.260), channel_id=1, source_target_pairs={{0,16},{16,32},{32,48},{48,64},{64,80},{80,96},{96,112},{112,128},... | collective-permute-start | bytes 11528 | tf_op jit(solution)/shard_map/ppermute | solution.py:17
  4.9 0.0 copy-done.7
  4.9 0.8 collective-permute-done
  5.7 0.1 maximum_convert_fusion
  5.8 0.0 copy-start.6
  5.8 0.0 copy-start.8
  5.8 0.0 copy-start.9
  5.8 0.0 copy-start.10
  5.9 0.0 copy-start.3
  5.9 1.5 %fusion.31 = (f32[256]{0:T(256)S(1)}, f32[256]{0:T(256)S(1)}, f32[64,256]{1,0:T(8,128)}) fusion(f32[64,286]{1,0:T(8,128)S(1)} %maximum_convert_fusion, f32[64]{0:T(128)S(1)} %get-tuple-element.37, f32[64]{0:T(128)S(1)} %get-tuple-element.38, f32[64]{0:T(128)S(1)} %get-tuple-element.9, f32[64]{0:T(128)S(1)} %get-tuple-element.10, ...), kind=kLoop, calls=%fused_computation.101 | loop fusion | flops 1048064 | bytes 2107136 | tf_op jit(solution)/shard_map/reduce_sum | solution.py:370
  7.4 0.0 copy-start.2
  7.4 0.6 broadcast_in_dim.4
  8.0 0.0 copy-start.1
  8.0 8.8 %all-to-all-start = ((f32[16,1,512]{2,1,0:T(1,128)}), f32[16,1,512]{2,1,0:T(1,128)}, u32[]{:S(2)}, u32[]{:S(2)}) async-start(f32[16,1,512]{2,1,0:T(1,128)} %broadcast_in_dim.4), calls=%async_computation | async-start | bytes 65536 | tf_op jit(solution)/shard_map/all_to_all | solution.py:22
  16.8 0.0 copy-done.6
  16.8 0.1 copy.22.ids_ref
  17.0 0.0 copy-done.8
  17.0 0.8 copy.23.logits_ref
  17.8 0.0 copy-done.9
  17.8 0.8 copy.24.prob_ref
  18.6 5.8 %all-to-all-done = f32[16,1,512]{2,1,0:T(1,128)} async-done(((f32[16,1,512]{2,1,0:T(1,128)}), f32[16,1,512]{2,1,0:T(1,128)}, u32[]{:S(2)}, u32[]{:S(2)}) %all-to-all-start) | async-done | bytes 32800 | tf_op jit(solution)/shard_map/all_to_all | solution.py:22
  24.4 0.8 reduce_sum.29
  25.2 0.0 copy-done.10
  25.2 0.9 multiply_convert_fusion
  26.1 16.3 %all_gather.3 = bf16[1024,256]{1,0:T(8,128)(2,1)S(1)} all-gather(bf16[64,256]{1,0:T(8,128)(2,1)S(1)} %multiply_convert_fusion), channel_id=1, replica_groups=mesh['sp'=32,'tp'=16] {'tp'}, dimensions={0}, use_global_device_ids=true | all-gather | bytes 557056 | tf_op jit(solution)/shard_map/all_gather | solution.py:377
  42.4 0.0 copy-done
  42.4 1.2 fusion.mixed_ref
  43.6 0.0 copy-done.3
  43.6 0.0 copy-done.2
  43.7 0.0 copy-done.1
  43.7 0.0 copy-start.4
  43.7 0.9 copy-done.4
  44.6 0.0 copy-start.5
  44.6 0.9 copy-done.5
  45.5 103.1 %shard_map.118 = bf16[256,128]{1,0:T(8,128)(2,1)S(1)} custom-call(bf16[256,128]{1,0:T(8,128)(2,1)S(1)} %fusion.mixed_ref, s32[256,2]{1,0:T(8,128)S(1)} %copy.22.ids_ref, s32[2,256]{1,0:T(2,128)S(1)} %bitcast.66, f32[256,2]{1,0:T(8,128)S(1)} %copy-done.4, f32[256,1]{1,0:T(8,128)S(1)} %copy-done.5, bf16[1,2048,256]{2,1,0:T(8,128)(2,1)S(1)} %copy-done.1, ...), custom_call_target="tpu_custom_call" | custom-call | tf_op jit(solution)/shard_map/pallas_call | solution.py:312
  148.6 0.6 copy.29
  (4 shorter events, 0.0 us)
Async XLA Ops:
  0.0 42.4 %copy-start = (bf16[1024,128]{1,0:T(8,128)(2,1)S(1)}, bf16[1024,128]{1,0:T(8,128)(2,1)}, u32[]{:S(2)}) copy-start(bf16[1024,128]{1,0:T(8,128)(2,1)} %param.16) | copy-start | bytes 786436
  0.9 4.0 %copy-start.7 = (f32[64,31]{0,1:T(8,128)S(1)}, f32[64,31]{0,1:T(8,128)}, u32[]{:S(2)}) copy-start(f32[64,31]{0,1:T(8,128)} %param.14) | copy-start | bytes 23812
  0.9 4.8 %collective-permute-start = (bf16[64,30]{1,0:T(8,128)(2,1)S(1)}, bf16[64,30]{1,0:T(8,128)(2,1)S(1)}, u32[]{:S(2)}, u32[]{:S(2)}) collective-permute-start(bf16[64,30]{1,0:T(8,128)(2,1)S(1)} %slice.260), channel_id=1, source_target_pairs={{0,16},{16,32},{32,48},{48,64},{64,80},{80,96},{96,112},{112,128},... | collective-permute-start | bytes 11528 | tf_op jit(solution)/shard_map/ppermute | solution.py:17
  5.8 11.0 %copy-start.6 = (s32[256,2]{0,1:T(2,128)S(1)}, s32[256,2]{0,1:T(2,128)}, u32[]{:S(2)}) copy-start(s32[256,2]{0,1:T(2,128)} %param.18) | copy-start | bytes 6148
  5.8 11.1 %copy-start.8 = (f32[256,2]{0,1:T(2,128)S(1)}, f32[256,2]{0,1:T(2,128)}, u32[]{:S(2)}) copy-start(f32[256,2]{0,1:T(2,128)} %param.19) | copy-start | bytes 6148
  5.8 11.9 %copy-start.9 = (f32[256]{0:T(256)S(1)}, f32[256]{0:T(256)}, u32[]{:S(2)}) copy-start(f32[256]{0:T(256)} %param.20) | copy-start | bytes 3076
  5.8 19.4 %copy-start.10 = (f32[64]{0:T(128)S(1)}, f32[64]{0:T(128)}, u32[]{:S(2)}) copy-start(f32[64]{0:T(128)} %param.15) | copy-start | bytes 772
  5.9 37.8 %copy-start.3 = (bf16[1,4096,128]{2,1,0:T(8,128)(2,1)S(1)}, bf16[1,4096,128]{2,1,0:T(8,128)(2,1)}, u32[]{:S(2)}) copy-start(bf16[1,4096,128]{2,1,0:T(8,128)(2,1)} %wd_hbm.1) | copy-start | bytes 3145732
  7.4 36.2 %copy-start.2 = (bf16[1,2048,256]{2,1,0:T(8,128)(2,1)S(1)}, bf16[1,2048,256]{2,1,0:T(8,128)(2,1)}, u32[]{:S(2)}) copy-start(bf16[1,2048,256]{2,1,0:T(8,128)(2,1)} %wu_hbm.1) | copy-start | bytes 3145732
  8.0 35.6 %copy-start.1 = (bf16[1,2048,256]{2,1,0:T(8,128)(2,1)S(1)}, bf16[1,2048,256]{2,1,0:T(8,128)(2,1)}, u32[]{:S(2)}) copy-start(bf16[1,2048,256]{2,1,0:T(8,128)(2,1)} %wg_hbm.1) | copy-start | bytes 3145732
  8.0 16.4 %all-to-all-start = ((f32[16,1,512]{2,1,0:T(1,128)}), f32[16,1,512]{2,1,0:T(1,128)}, u32[]{:S(2)}, u32[]{:S(2)}) async-start(f32[16,1,512]{2,1,0:T(1,128)} %broadcast_in_dim.4), calls=%async_computation | async-start | bytes 65536 | tf_op jit(solution)/shard_map/all_to_all | solution.py:22
  43.7 0.9 copy-start.4
  44.6 0.9 copy-start.5

commit v2 on v0

v2 whole, which is shorter than its diff:
```python
import functools
import jax
import jax.numpy as jnp
from jax import lax
from jax.experimental import pallas as pl
from jax.experimental.pallas import tpu as pltpu
from jax.sharding import PartitionSpec as P

BF = jnp.bfloat16
F32 = jnp.float32
MESH = pl.DeviceIdType.MESH
LANES = 128


def dot(a, b):
    return jnp.dot(a, b, preferred_element_type=F32)


def layer_kernel(
    dims,
    gv_hbm,
    gg_hbm,
    taps_ref,
    gain_ref,
    proj_hbm,
    resid_hbm,
    ids_ref,
    logits_ref,
    prob_ref,
    wg_hbm,
    wu_hbm,
    wd_hbm,
    out_ref,
    gv,
    gg,
    proj,
    resid,
    wg,
    wu,
    wd,
    wdt,
    tapcol,
    tail,
    halo,
    stats,
    act,
    pick,
    pick0,
    pick1,
    scales,
    mixed,
    outg,
    rows,
    own,
    give,
    take,
    sumout,
    sumin,
    res,
    ret,
    lsem,
    halo_s,
    halo_r,
    stat_s,
    stat_r,
    act_s,
    act_r,
    act_sib,
    wdt_s,
    wdt_r,
    dsend,
    drecv,
    rring,
    rsib,
    rsend,
    sib_s,
    sib_r,
    sum_s,
    sum_r,
    bsend,
    brecv,
):
    nx, nz, ny, cap, taps, channels = dims
    experts = nx * nz
    chunk = nx * cap
    tp = 2 * ny
    ha = ny // 2
    hb = ny - 1 - ha
    tokens, width = out_ref.shape
    own_ch = gv.shape[0]
    ffw = wg.shape[1]
    s = lax.axis_index("sp")
    j = lax.axis_index("tp")
    z, x = s // nx, s % nx
    y, c = j // 2, j % 2
    sib = 2 * y + (1 - c)

    def remote(src, dst, send, recv, where):
        pltpu.make_async_remote_copy(
            src_ref=src,
            dst_ref=dst,
            send_sem=send,
            recv_sem=recv,
            device_id=where,
            device_id_type=MESH,
        ).start()

    def arrived(ref, sem):
        pltpu.make_async_copy(ref, ref, sem).wait()

    def rows_of(n, size):
        return pl.ds(pl.multiple_of(n * size, size), size)

    loads = [
        pltpu.make_async_copy(a, b, lsem.at[n])
        for n, (a, b) in enumerate(
            (
                (gv_hbm, gv),
                (gg_hbm, gg),
                (wd_hbm.at[0], wd),
                (proj_hbm, proj),
                (resid_hbm, resid),
                (wg_hbm.at[0], wg),
                (wu_hbm.at[0], wu),
            )
        )
    ]
    for load in loads:
        load.start()

    barrier = pltpu.get_barrier_semaphore()

    def greet_sp(k, carry):
        pl.semaphore_signal(barrier, inc=1, device_id=((s + k) % experts, j), device_id_type=MESH)
        return carry

    def greet_tp(k, carry):
        pl.semaphore_signal(barrier, inc=1, device_id=(s, (j + k) % tp), device_id_type=MESH)
        return carry

    lax.fori_loop(1, experts, greet_sp, 0)
    lax.fori_loop(1, tp, greet_tp, 0)

    loads[0].wait()
    loads[1].wait()
    gated = (gv[...].astype(F32) * jax.nn.sigmoid(gg[...].astype(F32))).astype(BF)
    tail[...] = gated[:, tokens - LANES :]

    id0 = ids_ref[0:1, :]
    id1 = ids_ref[1:2, :]
    e_io = lax.broadcasted_iota(jnp.int32, (experts, tokens), 0)
    named = jnp.where((e_io == id0) | (e_io == id1), 1.0, 0.0)
    r_io = lax.broadcasted_iota(jnp.int32, (tokens, tokens), 0)
    c_io = lax.broadcasted_iota(jnp.int32, (tokens, tokens), 1)
    upper = jnp.where(r_io < c_io, 1.0, 0.0).astype(BF)
    before = dot(named.astype(BF), upper)
    slot0 = jnp.sum(jnp.where(e_io == id0, before, 0.0), axis=0, keepdims=True) + id0.astype(F32) * cap
    slot1 = jnp.sum(jnp.where(e_io == id1, before, 0.0), axis=0, keepdims=True) + id1.astype(F32) * cap
    s_io = lax.broadcasted_iota(jnp.int32, (experts * cap, tokens), 0).astype(F32)
    pick[...] = jnp.where((s_io == slot0) | (s_io == slot1), 1.0, 0.0).astype(BF)
    l0 = logits_ref[0:1, :]
    l1 = logits_ref[1:2, :]
    top = jnp.maximum(l0, l1)
    e0 = jnp.exp(l0 - top)
    e1 = jnp.exp(l1 - top)
    scale = prob_ref[...] / (e0 + e1)
    k_io = lax.broadcasted_iota(jnp.int32, (8, tokens), 0)
    stack = jnp.where(
        k_io == 0, slot0, jnp.where(k_io == 1, slot1, jnp.where(k_io == 2, e0 * scale, e1 * scale))
    )
    cols = stack.T
    scales[...] = cols
    t_io = lax.broadcasted_iota(jnp.int32, (tokens, experts * cap), 1).astype(F32)
    pick0[...] = jnp.where(t_io == cols[:, 0:1], 1.0, 0.0).astype(BF)
    pick1[...] = jnp.where(t_io == cols[:, 1:2], 1.0, 0.0).astype(BF)
    tapcol[...] = jnp.zeros_like(tapcol)
    tapcol[0:taps, 0:own_ch] = taps_ref[...]
    tapcol[taps : taps + 1, 0:own_ch] = gain_ref[...]
    tap = tapcol[...].T

    loads[2].wait()
    wdt[j] = wd[rows_of(j, ffw), :]

    pl.semaphore_wait(barrier, experts - 1 + tp - 1)

    def give_wd(peer_y, peer_c):
        peer = 2 * peer_y + peer_c
        remote(wd.at[rows_of(peer, ffw), :], wdt.at[j], wdt_s, wdt_r, (s, peer))

    def give_wd_at(reach):
        for d in sorted({reach % ny, (ny - reach) % ny}):
            give_wd((y + d) % ny, c)
            give_wd((y + d) % ny, 1 - c)

    @pl.when(s < experts - 1)
    def _():
        remote(tail, halo, halo_s, halo_r, ((s + 1) % experts, j))

    give_wd(y, 1 - c)
    give_wd_at(1)

    @pl.when(s == 0)
    def _():
        halo[...] = jnp.zeros_like(halo)

    @pl.when(s > 0)
    def _():
        arrived(halo, halo_r)

    padded = jnp.concatenate([halo[...], gated], axis=1).astype(F32)
    filtered = jnp.zeros((own_ch, tokens), F32)
    for o in range(taps):
        shift = taps - 1 - o
        moved = pltpu.roll(padded, shift, 1) if shift else padded
        filtered = filtered + tap[0:own_ch, o : o + 1] * moved[:, LANES:]
    stats[j, 0:1, :] = jnp.sum(filtered, axis=0, keepdims=True)
    stats[j, 1:2, :] = jnp.sum(filtered * filtered, axis=0, keepdims=True)

    def give_stats(k, carry):
        remote(stats.at[j], stats.at[j], stat_s, stat_r, (s, (j + k) % tp))
        return carry

    lax.fori_loop(1, tp, give_stats, 0)
    if ny > 2:
        give_wd_at(2)
    arrived(stats.at[pl.ds(0, tp - 1)], stat_r)
    totals = jnp.sum(stats[...], axis=0)
    mean = totals[0:1] / channels
    var = totals[1:2] / channels - mean * mean
    normed = (filtered - mean) * lax.rsqrt(var + 1e-05) * tap[0:own_ch, taps : taps + 1]
    act[j] = (normed / (1.0 + jnp.exp(-normed))).astype(BF)

    near = []
    for d in range(1, ha + 1):
        near.append(d)
        if ny - d != d:
            near.append(ny - d)
    for d in near:
        remote(act.at[j], act.at[j], act_s, act_r.at[d], (s, 2 * ((y + d) % ny) + c))
    remote(act.at[j], act.at[j], act_s, act_sib, (s, sib))
    for reach in range(3, ha + 1):
        give_wd_at(reach)
    for d in near:
        k = 2 * ((y + ny - d) % ny) + c
        arrived(act.at[k], act_r.at[d])
        remote(act.at[k], act.at[k], act_s, act_sib, (s, sib))
    arrived(act.at[pl.ds(0, ny)], act_sib)
    loads[3].wait()
    loads[4].wait()
    projected = lax.dot_general(
        act[...].reshape(tp * own_ch, tokens),
        proj[...],
        (((0,), (0,)), ((), ())),
        preferred_element_type=F32,
    )
    mixed[...] = (resid[...].astype(F32) + projected).astype(BF)

    outg[...] = dot(pick[...], mixed[...]).astype(BF)
    rows[z, j, rows_of(x, cap), :] = outg[rows_of(s, cap), :]

    def offset(i):
        return ((i + 1) // 2) * (1 - 2 * ((i + 1) % 2))

    def dispatch(n, carry):
        i, dx = n // nx, n % nx
        e = ((z - offset(i) + nz) % nz) * nx + (x + dx) % nx
        remote(
            outg.at[rows_of(e, cap), :],
            rows.at[z, j, rows_of(x, cap), :],
            dsend,
            drecv.at[z],
            (e, j),
        )
        return carry

    lax.fori_loop(1, experts, dispatch, 0)

    def push(q, i, origin_y, hop, leg, sgn):
        ref = rows.at[q, 2 * origin_y + c]
        step = sgn * (1 - 2 * leg)
        where = (s, 2 * ((y + step + ny) % ny) + c)
        remote(ref, ref, rsend.at[i], rring.at[i, leg * ha + hop], where)

    def share(q, i, origin_y):
        ref = rows.at[q, 2 * origin_y + c]
        remote(ref, ref, rsend.at[i], rsib.at[i], (s, sib))

    def tick(t, carry):
        def at(stage, body):
            i = t - stage

            @pl.when((i >= 0) & (i < nz))
            def _():
                body(i, (z + offset(i) + nz) % nz, 1 - 2 * (i % 2))

        def rows_open(i, q, sgn):
            @pl.when(i == 0)
            def _():
                if nx > 1:
                    arrived(outg.at[pl.ds(0, (nx - 1) * cap), :], drecv.at[q])

            @pl.when(i > 0)
            def _():
                arrived(outg.at[pl.ds(0, nx * cap), :], drecv.at[q])

            push(q, i, y, 0, 0, sgn)
            if hb > 0:
                push(q, i, y, 0, 1, sgn)
            share(q, i, y)

        def rows_hop(h, i, q, sgn):
            for leg, reach in ((0, ha), (1, hb)):
                if h > reach:
                    continue
                origin = (y - sgn * (1 - 2 * leg) * h + 2 * ny) % ny
                arrived(rows.at[q, 2 * origin + c], rring.at[i, leg * ha + h - 1])
                if h < reach:
                    push(q, i, origin, h, leg, sgn)
                share(q, i, origin)

        def expert(i, q, sgn):
            @pl.when(i == 0)
            def _():
                loads[5].wait()
                loads[6].wait()
                arrived(wd.at[pl.ds(0, (tp - 1) * ffw), :], wdt_r)

            arrived(rows.at[q, pl.ds(0, ny)], rsib.at[i])
            r = jnp.concatenate([rows[q, b] for b in range(tp)], axis=1)
            g = dot(r, wg[...])
            u = dot(r, wu[...])
            h = ((g / (1.0 + jnp.exp(-g))) * u).astype(BF)
            for b in range(ny):
                w = jnp.concatenate([wdt[2 * b + c], wdt[2 * b + 1 - c]], axis=1)
                part = dot(h, w)
                own[i, b] = part[:, :width]
                give[i, b] = part[:, width:].astype(BF)
            remote(give.at[i], take.at[i], sib_s.at[i], sib_r.at[i], (s, sib))

        def mine(i, b):
            return own[i, b] + take[i, b].astype(F32)

        def sum_hop(m, i, q, sgn):
            if m == 1:
                arrived(take.at[i], sib_r.at[i])
            for leg, reach in ((0, ha), (1, hb)):
                if m > reach:
                    continue
                step = sgn * (1 - 2 * leg)
                k = reach - m + 1
                n = leg * ha + m - 1
                total = mine(i, (y + step * k + 2 * ny) % ny)
                if m > 1:
                    arrived(sumin.at[i, n - 1], sum_r.at[i, n - 1])
                    total = total + sumin[i, n - 1].astype(F32)
                sumout[i, n] = total.astype(BF)
                where = (s, 2 * ((y + step + ny) % ny) + c)
                remote(sumout.at[i, n], sumin.at[i, n], sum_s.at[i], sum_r.at[i, n], where)

        def finish(i, q, sgn):
            total = mine(i, y)
            for n in ([ha - 1, ny - 2] if hb > 0 else [ha - 1]):
                arrived(sumin.at[i, n], sum_r.at[i, n])
                total = total + sumin[i, n].astype(F32)
            res[i] = total.astype(BF)
            for xt in range(nx):
                tgt = q * nx + xt

                @pl.when(tgt == s)
                def _():
                    ret[rows_of(s, cap), :] = res[i, pl.ds(xt * cap, cap), :]

                @pl.when(tgt != s)
                def _():
                    remote(
                        res.at[i, pl.ds(xt * cap, cap), :],
                        ret.at[rows_of(s, cap), :],
                        bsend,
                        brecv,
                        (tgt, j),
                    )

        at(0, rows_open)
        for h in range(1, ha + 1):
            at(h, functools.partial(rows_hop, h))
        for m in range(1, ha + 1):
            at(ha + 1 + m, functools.partial(sum_hop, m))
        at(2 * ha + 2, finish)
        at(ha + 1, expert)
        return carry

    lax.fori_loop(0, nz + 2 * ha + 2, tick, 0)

    far = outg.at[pl.ds(0, (experts - 1) * cap), :]
    arrived(far, brecv)
    back = ret[...]
    routed = dot(pick0[...], back) * scales[:, 2:3] + dot(pick1[...], back) * scales[:, 3:4]
    out_ref[...] = (mixed[...].astype(F32) + routed).astype(BF)

    @pl.when(s < experts - 1)
    def _():
        arrived(halo, halo_s)

    arrived(wd.at[pl.ds(0, (tp - 1) * ffw), :], wdt_s)
    arrived(stats.at[pl.ds(0, tp - 1)], stat_s)
    arrived(act.at[pl.ds(0, 2 * ny - 1)], act_s)
    arrived(far, dsend)
    arrived(far, bsend)

    def drain(i, carry):
        arrived(rows.at[0, pl.ds(0, tp - 1)], rsend.at[i])
        arrived(give.at[0], sib_s.at[i])
        arrived(sumout.at[0], sum_s.at[i])
        return carry

    lax.fori_loop(0, nz, drain, 0)


def per_device(
    glu_value,
    glu_gate,
    conv_taps,
    norm_gain,
    out_proj,
    resid,
    expert_ids,
    route_logits,
    group_prob,
    w_gate,
    w_up,
    w_down,
):
    sp, tp = lax.axis_size("sp"), lax.axis_size("tp")
    nx = 4 if sp % 8 == 0 else 1
    nz, ny = sp // nx, tp // 2
    tokens, width = resid.shape
    cap = 4 * tokens // sp
    depth, ffw = w_gate.shape[1:]
    own_ch, taps = conv_taps.shape
    chunk = nx * cap
    dma = pltpu.SemaphoreType.DMA
    vmem = pl.BlockSpec(memory_space=pltpu.VMEM)
    hbm = pl.BlockSpec(memory_space=pl.ANY)
    dims = (nx, nz, ny, cap, taps, own_ch * tp)
    return pl.pallas_call(
        functools.partial(layer_kernel, dims),
        out_shape=jax.ShapeDtypeStruct((tokens, width), BF),
        in_specs=[hbm, hbm, vmem, vmem, hbm, hbm, vmem, vmem, vmem, hbm, hbm, hbm],
        out_specs=vmem,
        scratch_shapes=[
            pltpu.VMEM(glu_value.shape, BF),
            pltpu.VMEM(glu_gate.shape, BF),
            pltpu.VMEM(out_proj.shape, BF),
            pltpu.VMEM(resid.shape, BF),
            pltpu.VMEM((depth, ffw), BF),
            pltpu.VMEM((depth, ffw), BF),
            pltpu.VMEM(w_down.shape[1:], BF),
            pltpu.VMEM((tp, ffw, width), BF),
            pltpu.VMEM((32, LANES), F32),
            pltpu.VMEM((own_ch, LANES), BF),
            pltpu.VMEM((own_ch, LANES), BF),
            pltpu.VMEM((tp, 2, tokens), F32),
            pltpu.VMEM((tp, own_ch, tokens), BF),
            pltpu.VMEM((sp * cap, tokens), BF),
            pltpu.VMEM((tokens, sp * cap), BF),
            pltpu.VMEM((tokens, sp * cap), BF),
            pltpu.VMEM((tokens, 8), F32),
            pltpu.VMEM((tokens, width), BF),
            pltpu.VMEM((sp * cap, width), BF),
            pltpu.VMEM((nz, tp, chunk, width), BF),
            pltpu.VMEM((nz, ny, chunk, width), F32),
            pltpu.VMEM((nz, ny, chunk, width), BF),
            pltpu.VMEM((nz, ny, chunk, width), BF),
            pltpu.VMEM((nz, ny - 1, chunk, width), BF),
            pltpu.VMEM((nz, ny - 1, chunk, width), BF),
            pltpu.VMEM((nz, chunk, width), BF),
            pltpu.VMEM((sp * cap, width), BF),
            dma((7,)),
            dma(()),
            dma(()),
            dma(()),
            dma(()),
            dma(()),
            dma((ny,)),
            dma(()),
            dma(()),
            dma(()),
            dma(()),
            dma((nz,)),
            dma((nz, ny - 1)),
            dma((nz,)),
            dma((nz,)),
            dma((nz,)),
            dma((nz,)),
            dma((nz,)),
            dma((nz, ny - 1)),
            dma(()),
            dma(()),
        ],
        compiler_params=pltpu.CompilerParams(
            collective_id=0, has_side_effects=True, vmem_limit_bytes=63 * 1024 * 1024
        ),
    )(
        glu_value,
        glu_gate,
        conv_taps.T,
        norm_gain[None, :],
        out_proj,
        resid,
        expert_ids.T,
        route_logits.T,
        group_prob[None, :],
        w_gate,
        w_up,
        w_down,
    )


def solution(mesh):
    return jax.shard_map(
        per_device,
        mesh=mesh,
        in_specs=(
            P("tp", "sp"),
            P("tp", "sp"),
            P("tp", None),
            P("tp"),
            P(None, "tp"),
            P("sp", "tp"),
            P("sp", None),
            P("sp", None),
            P("sp"),
            P("sp", None, "tp"),
            P("sp", None, "tp"),
            P("sp", None, "tp"),
        ),
        out_specs=P("sp", "tp"),
        check_vma=False,
    )
```

time: 239 us -> 111 us (0.46)
  waiting for transfers between devices: 130 us -> 0 us
  Pallas kernels: 0 us -> 107 us
  blocking collectives: 40.6 us -> 0 us
  starting transfers between devices: 18.9 us -> 0 us
  between operations: 13.7 us -> 0.01 us
  local copies, waits for them, and re-layouts: 14.4 us -> 1.47 us
  matrix products: 12.7 us -> 0 us
  other arithmetic: 7.23 us -> 0 us
    all_gather x2 -> x0, waiting for transfers between devices: 114 us -> none  [the longest x1 67.3 us: per_device(): lax.all_gather(hidden, 'tp', axis=1, tiled=True)]
    pallas_call x0 -> x1, Pallas kernels: none -> 107 us  [per_device(): pl.pallas_call(functools.partial(layer_kernel, dims), out_shape=jax.Shape...]
    all_to_all x1 -> x0, blocking collectives: 24.3 us -> none  [per_device(): lax.all_to_all(outgoing, 'sp', split_axis=0, concat_axis=0, tiled=True)]
    all_gather x1 -> x0, blocking collectives: 16.3 us -> none  [per_device(): lax.all_gather(activated, 'tp', axis=0, tiled=True)]
    all_to_all x2 -> x0, waiting for transfers between devices: 15.9 us -> none  [the longest x1 11.2 us: per_device(): lax.all_to_all(results, 'sp', split_axis=0, concat_axis=0, tiled=True)]
    all_to_all x2 -> x0, starting transfers between devices: 14.9 us -> none  [the longest x1 8.07 us: from_everyone(): return lax.all_to_all(copies, axis, split_axis=0, concat_axis=0, tiled=True)]
    dot_general x4 -> x0, matrix products: 12.7 us -> none  [the longest x1 6.65 us: per_device(): jnp.dot(lax.all_gather(hidden, 'tp', axis=1, tiled=True), weights, prefer...]
    scatter x2 -> x0, local copies, waits for them, and re-layouts: 4.89 us -> none  [the longest x1 2.45 us: per_device(): filled = jnp.zeros((experts * capacity,), jnp.bool_).at[slot].set(True)]
  transfers between devices with their start and end apart: 5 -> 0, of which waited for: 4 -> 0; matrix products, arithmetic and copies ran while one was open for 5% -> 0% of each run, Pallas kernels for 0% -> 0%
where the time goes in v2:
time: 111 us; the launch traced here: 109 us
  Pallas kernels  107 us (96%)
  local copies, waits for them, and re-layouts  1.47 us (1%)
    pallas_call x1, Pallas kernels, per_device(): pl.pallas_call(functools.partial(layer_kernel, dims), out_shape=jax.Shape...  107 us

profile of v2, /device:TPU:1, one launch (start us, length us, event | category | flops | bytes accessed | tf_op | source)
XLA Modules:
  0.0 108.8 jit_solution(16688632687051030350)
XLA Ops:
  0.0 107.4 %shard_map.118 = bf16[256,128]{1,0:T(8,128)(2,1)} custom-call(bf16[64,256]{1,0:T(8,128)(2,1)} %gv_hbm.1, bf16[64,256]{1,0:T(8,128)(2,1)} %gg_hbm.1, f32[31,64]{1,0:T(8,128)} %bitcast.5, f32[1,64]{1,0:T(1,128)} %bitcast.9, bf16[1024,128]{1,0:T(8,128)(2,1)} %proj_hbm.1, bf16[256,128]{1,0:T(8,128)(2,1)} %resid_hbm.1, s32[2,256]{1,0:T(2,128)} %bitcast.6, ...), custom_call_target="tpu_custom_call" | custom-call | tf_op jit(solution)/shard_map/pallas_call | solution.py:445
  107.4 1.5 %copy.14 = bf16[256,128]{1,0:T(8,128)(2,1)} copy(bf16[256,128]{1,0:T(8,128)(2,1)} %shard_map.118) | data formatting | bytes 131072

commit v3 on v2

--- a/solution.py
+++ b/solution.py
@@ -258,12 +258,9 @@
     outg[...] = dot(pick[...], mixed[...]).astype(BF)
     rows[z, j, rows_of(x, cap), :] = outg[rows_of(s, cap), :]
 
-    def offset(i):
-        return ((i + 1) // 2) * (1 - 2 * ((i + 1) % 2))
-
     def dispatch(n, carry):
         i, dx = n // nx, n % nx
-        e = ((z - offset(i) + nz) % nz) * nx + (x + dx) % nx
+        e = ((z - i + nz) % nz) * nx + (x + dx) % nx
         remote(
             outg.at[rows_of(e, cap), :],
             rows.at[z, j, rows_of(x, cap), :],
@@ -287,11 +284,11 @@
 
     def tick(t, carry):
         def at(stage, body):
-            i = t - stage
+            i = t - 2 * stage
 
             @pl.when((i >= 0) & (i < nz))
             def _():
-                body(i, (z + offset(i) + nz) % nz, 1 - 2 * (i % 2))
+                body(i, (z + i) % nz, 1 - 2 * (i % 2))
 
         def rows_open(i, q, sgn):
             @pl.when(i == 0)
@@ -389,7 +386,7 @@
         at(ha + 1, expert)
         return carry
 
-    lax.fori_loop(0, nz + 2 * ha + 2, tick, 0)
+    lax.fori_loop(0, nz + 2 * (2 * ha + 2), tick, 0)
 
     far = outg.at[pl.ds(0, (experts - 1) * cap), :]
     arrived(far, brecv)

time: 111 us -> 103 us (0.928)
  Pallas kernels: 107 us -> 100 us
    pallas_call x1, Pallas kernels: 107 us -> 100 us  [per_device(): pl.pallas_call(functools.partial(layer_kernel, dims), out_shape=jax.Shape...]
where the time goes in v3:
time: 103 us; the launch traced here: 101 us
  Pallas kernels  100 us (97%)
  local copies, waits for them, and re-layouts  1.47 us (1%)
    pallas_call x1, Pallas kernels, per_device(): pl.pallas_call(functools.partial(layer_kernel, dims), out_shape=jax.Shape...  100 us

profile of v3, /device:TPU:1, one launch (start us, length us, event | category | flops | bytes accessed | tf_op | source)
XLA Modules:
  0.0 101.4 jit_solution(18416964014044385228)
XLA Ops:
  0.0 100.0 %shard_map.118 = bf16[256,128]{1,0:T(8,128)(2,1)} custom-call(bf16[64,256]{1,0:T(8,128)(2,1)} %gv_hbm.1, bf16[64,256]{1,0:T(8,128)(2,1)} %gg_hbm.1, f32[31,64]{1,0:T(8,128)} %bitcast.5, f32[1,64]{1,0:T(1,128)} %bitcast.9, bf16[1024,128]{1,0:T(8,128)(2,1)} %proj_hbm.1, bf16[256,128]{1,0:T(8,128)(2,1)} %resid_hbm.1, s32[2,256]{1,0:T(2,128)} %bitcast.6, ...), custom_call_target="tpu_custom_call" | custom-call | tf_op jit(solution)/shard_map/pallas_call | solution.py:442
  100.0 1.5 %copy.14 = bf16[256,128]{1,0:T(8,128)(2,1)} copy(bf16[256,128]{1,0:T(8,128)(2,1)} %shard_map.118) | data formatting | bytes 131072

commit v4 on v3

--- a/solution.py
+++ b/solution.py
@@ -66,6 +66,9 @@
     act_s,
     act_r,
     act_sib,
+    relay,
+    relay_s,
+    relay_r,
     wdt_s,
     wdt_r,
     dsend,
@@ -91,8 +94,8 @@
     ffw = wg.shape[1]
     s = lax.axis_index("sp")
     j = lax.axis_index("tp")
-    z, x = s // nx, s % nx
-    y, c = j // 2, j % 2
+    z, x = lax.div(s, nx), lax.rem(s, nx)
+    y, c = lax.div(j, 2), lax.rem(j, 2)
     sib = 2 * y + (1 - c)
 
     def remote(src, dst, send, recv, where):
@@ -130,16 +133,13 @@
 
     barrier = pltpu.get_barrier_semaphore()
 
-    def greet_sp(k, carry):
-        pl.semaphore_signal(barrier, inc=1, device_id=((s + k) % experts, j), device_id_type=MESH)
-        return carry
-
-    def greet_tp(k, carry):
-        pl.semaphore_signal(barrier, inc=1, device_id=(s, (j + k) % tp), device_id_type=MESH)
-        return carry
-
-    lax.fori_loop(1, experts, greet_sp, 0)
-    lax.fori_loop(1, tp, greet_tp, 0)
+    for k in sorted(range(1, experts), key=lambda k: -min(k // nx, nz - k // nx)):
+        peer = (lax.rem(s + k, experts), j)
+        pl.semaphore_signal(barrier, inc=1, device_id=peer, device_id_type=MESH)
+    far_first = sorted(range(1, tp), key=lambda k: -min(k // 2, ny - k // 2))
+    for k in far_first:
+        peer = (s, lax.rem(j + k, tp))
+        pl.semaphore_signal(barrier, inc=1, device_id=peer, device_id_type=MESH)
 
     loads[0].wait()
     loads[1].wait()
@@ -192,6 +192,21 @@
             give_wd((y + d) % ny, c)
             give_wd((y + d) % ny, 1 - c)
 
+    halfway = ny // 4
+    lean = 1 - 2 * c
+    before_y, after_y = (y - lean * halfway + ny) % ny, (y + lean * halfway + ny) % ny
+    across = (y + ha) % ny
+
+    def give_wd_across():
+        for n, peer_c in enumerate((c, 1 - c)):
+            block = wd.at[rows_of(2 * across + peer_c, ffw), :]
+            remote(block, relay.at[n], relay_s, relay_r, (s, 2 * after_y + c))
+
+    def relay_wd():
+        arrived(relay, relay_r)
+        for n, peer_c in enumerate((c, 1 - c)):
+            remote(relay.at[n], wdt.at[2 * before_y + c], wdt_s, wdt_r, (s, 2 * after_y + peer_c))
+
     @pl.when(s < experts - 1)
     def _():
         remote(tail, halo, halo_s, halo_r, ((s + 1) % experts, j))
@@ -216,13 +231,10 @@
     stats[j, 0:1, :] = jnp.sum(filtered, axis=0, keepdims=True)
     stats[j, 1:2, :] = jnp.sum(filtered * filtered, axis=0, keepdims=True)
 
-    def give_stats(k, carry):
-        remote(stats.at[j], stats.at[j], stat_s, stat_r, (s, (j + k) % tp))
-        return carry
-
-    lax.fori_loop(1, tp, give_stats, 0)
-    if ny > 2:
-        give_wd_at(2)
+    for k in far_first:
+        remote(stats.at[j], stats.at[j], stat_s, stat_r, (s, lax.rem(j + k, tp)))
+    for reach in range(2, ha - 1):
+        give_wd_at(reach)
     arrived(stats.at[pl.ds(0, tp - 1)], stat_r)
     totals = jnp.sum(stats[...], axis=0)
     mean = totals[0:1] / channels
@@ -230,20 +242,41 @@
     normed = (filtered - mean) * lax.rsqrt(var + 1e-05) * tap[0:own_ch, taps : taps + 1]
     act[j] = (normed / (1.0 + jnp.exp(-normed))).astype(BF)
 
-    near = []
-    for d in range(1, ha + 1):
-        near.append(d)
-        if ny - d != d:
-            near.append(ny - d)
-    for d in near:
-        remote(act.at[j], act.at[j], act_s, act_r.at[d], (s, 2 * ((y + d) % ny) + c))
+    def act_from(d):
+        return act.at[2 * ((y - d + 2 * ny) % ny) + c]
+
+    def send_act(d, reach):
+        ref = act_from(d)
+        remote(ref, ref, act_s, act_r.at[(d + reach) % ny], (s, 2 * ((y + reach + ny) % ny) + c))
+
+    def share_act(d):
+        ref = act_from(d)
+        arrived(ref, act_r.at[d % ny])
+        remote(ref, ref, act_s, act_sib, (s, sib))
+
+    for reach in range(halfway, 0, -1):
+        send_act(0, reach)
+        send_act(0, -reach)
     remote(act.at[j], act.at[j], act_s, act_sib, (s, sib))
-    for reach in range(3, ha + 1):
-        give_wd_at(reach)
-    for d in near:
-        k = 2 * ((y + ny - d) % ny) + c
-        arrived(act.at[k], act_r.at[d])
-        remote(act.at[k], act.at[k], act_s, act_sib, (s, sib))
+    for side in (1, -1):
+        share_act(side * halfway)
+        for reach in range(1, halfway):
+            send_act(side * halfway, side * reach)
+
+        @pl.when(lean == side)
+        def _():
+            send_act(side * halfway, side * halfway)
+
+    give_wd_across()
+    if ha > 2:
+        give_wd_at(ha - 1)
+    for d in range(1, halfway):
+        share_act(d)
+        share_act(-d)
+    for d in range(halfway + 1, ha):
+        share_act(d)
+        share_act(-d)
+    share_act(ha)
     arrived(act.at[pl.ds(0, ny)], act_sib)
     loads[3].wait()
     loads[4].wait()
@@ -256,41 +289,45 @@
     mixed[...] = (resid[...].astype(F32) + projected).astype(BF)
 
     outg[...] = dot(pick[...], mixed[...]).astype(BF)
-    rows[z, j, rows_of(x, cap), :] = outg[rows_of(s, cap), :]
-
-    def dispatch(n, carry):
-        i, dx = n // nx, n % nx
-        e = ((z - i + nz) % nz) * nx + (x + dx) % nx
-        remote(
-            outg.at[rows_of(e, cap), :],
-            rows.at[z, j, rows_of(x, cap), :],
-            dsend,
-            drecv.at[z],
-            (e, j),
-        )
-        return carry
-
-    lax.fori_loop(1, experts, dispatch, 0)
-
-    def push(q, i, origin_y, hop, leg, sgn):
-        ref = rows.at[q, 2 * origin_y + c]
-        step = sgn * (1 - 2 * leg)
-        where = (s, 2 * ((y + step + ny) % ny) + c)
-        remote(ref, ref, rsend.at[i], rring.at[i, leg * ha + hop], where)
-
-    def share(q, i, origin_y):
-        ref = rows.at[q, 2 * origin_y + c]
-        remote(ref, ref, rsend.at[i], rsib.at[i], (s, sib))
+    rows[z, c, y, rows_of(x, cap), :] = outg[rows_of(s, cap), :]
+
+    for i in range(nz):
+        zt = lax.rem(z + (nz - i), nz)
+        for dx in range(nx):
+            if i + dx == 0:
+                continue
+            e = zt * nx + lax.rem(x + dx, nx)
+            remote(
+                outg.at[rows_of(e, cap), :],
+                rows.at[z, c, y, rows_of(x, cap), :],
+                dsend,
+                drecv.at[z],
+                (e, j),
+            )
+
+    relay_wd()
+    above = 2 * lax.rem(y + 1, ny) + c
+    below = 2 * lax.rem(y + (ny - 1), ny) + c
+
+    def toward(odd, leg):
+        return (s, above + (odd if leg == 0 else 1 - odd) * (below - above))
+
+    def chip(step, k):
+        return lax.rem(y + step * k + ny, ny)
+
+    def push(q, i, origin_y, hop, leg, odd):
+        ref = rows.at[q, c, origin_y]
+        remote(ref, ref, rsend.at[i], rring.at[i, leg * ha + hop], toward(odd, leg))
 
     def tick(t, carry):
         def at(stage, body):
-            i = t - 2 * stage
+            i = t - stage
 
             @pl.when((i >= 0) & (i < nz))
             def _():
-                body(i, (z + i) % nz, 1 - 2 * (i % 2))
-
-        def rows_open(i, q, sgn):
+                body(i, lax.rem(z + i, nz), lax.rem(i, 2))
+
+        def rows_open(i, q, odd):
             @pl.when(i == 0)
             def _():
                 if nx > 1:
@@ -300,30 +337,30 @@
             def _():
                 arrived(outg.at[pl.ds(0, nx * cap), :], drecv.at[q])
 
-            push(q, i, y, 0, 0, sgn)
+            push(q, i, y, 0, 0, odd)
             if hb > 0:
-                push(q, i, y, 0, 1, sgn)
-            share(q, i, y)
-
-        def rows_hop(h, i, q, sgn):
+                push(q, i, y, 0, 1, odd)
+
+        def rows_hop(h, i, q, odd):
             for leg, reach in ((0, ha), (1, hb)):
                 if h > reach:
                     continue
-                origin = (y - sgn * (1 - 2 * leg) * h + 2 * ny) % ny
-                arrived(rows.at[q, 2 * origin + c], rring.at[i, leg * ha + h - 1])
+                origin = chip((2 * odd - 1) * (1 - 2 * leg), h)
+                arrived(rows.at[q, c, origin], rring.at[i, leg * ha + h - 1])
                 if h < reach:
-                    push(q, i, origin, h, leg, sgn)
-                share(q, i, origin)
-
-        def expert(i, q, sgn):
+                    push(q, i, origin, h, leg, odd)
+            if h == ha:
+                remote(rows.at[q, c], rows.at[q, c], rsend.at[i], rsib.at[i], (s, sib))
+
+        def expert(i, q, odd):
             @pl.when(i == 0)
             def _():
                 loads[5].wait()
                 loads[6].wait()
                 arrived(wd.at[pl.ds(0, (tp - 1) * ffw), :], wdt_r)
 
-            arrived(rows.at[q, pl.ds(0, ny)], rsib.at[i])
-            r = jnp.concatenate([rows[q, b] for b in range(tp)], axis=1)
+            arrived(rows.at[q, 0], rsib.at[i])
+            r = jnp.concatenate([rows[q, b % 2, b // 2] for b in range(tp)], axis=1)
             g = dot(r, wg[...])
             u = dot(r, wu[...])
             h = ((g / (1.0 + jnp.exp(-g))) * u).astype(BF)
@@ -337,24 +374,23 @@
         def mine(i, b):
             return own[i, b] + take[i, b].astype(F32)
 
-        def sum_hop(m, i, q, sgn):
+        def sum_hop(m, i, q, odd):
             if m == 1:
                 arrived(take.at[i], sib_r.at[i])
             for leg, reach in ((0, ha), (1, hb)):
                 if m > reach:
                     continue
-                step = sgn * (1 - 2 * leg)
                 k = reach - m + 1
                 n = leg * ha + m - 1
-                total = mine(i, (y + step * k + 2 * ny) % ny)
+                total = mine(i, chip((1 - 2 * odd) * (1 - 2 * leg), k))
                 if m > 1:
                     arrived(sumin.at[i, n - 1], sum_r.at[i, n - 1])
                     total = total + sumin[i, n - 1].astype(F32)
                 sumout[i, n] = total.astype(BF)
-                where = (s, 2 * ((y + step + ny) % ny) + c)
-                remote(sumout.at[i, n], sumin.at[i, n], sum_s.at[i], sum_r.at[i, n], where)
-
-        def finish(i, q, sgn):
+                ref = sumout.at[i, n]
+                remote(ref, sumin.at[i, n], sum_s.at[i], sum_r.at[i, n], toward(odd, leg))
+
+        def finish(i, q, odd):
             total = mine(i, y)
             for n in ([ha - 1, ny - 2] if hb > 0 else [ha - 1]):
                 arrived(sumin.at[i, n], sum_r.at[i, n])
@@ -377,16 +413,17 @@
                         (tgt, j),
                     )
 
+        last = 2 * ha + 2
+        at(2 * last - 2, finish)
+        for m in range(ha, 0, -1):
+            at(last + 2 * (m - 1), functools.partial(sum_hop, m))
+        for h in range(ha, 0, -1):
+            at(2 * h, functools.partial(rows_hop, h))
         at(0, rows_open)
-        for h in range(1, ha + 1):
-            at(h, functools.partial(rows_hop, h))
-        for m in range(1, ha + 1):
-            at(ha + 1 + m, functools.partial(sum_hop, m))
-        at(2 * ha + 2, finish)
-        at(ha + 1, expert)
+        at(last - 1, expert)
         return carry
 
-    lax.fori_loop(0, nz + 2 * (2 * ha + 2), tick, 0)
+    lax.fori_loop(0, nz + 4 * ha + 2, tick, 0)
 
     far = outg.at[pl.ds(0, (experts - 1) * cap), :]
     arrived(far, brecv)
@@ -399,13 +436,15 @@
         arrived(halo, halo_s)
 
     arrived(wd.at[pl.ds(0, (tp - 1) * ffw), :], wdt_s)
+    arrived(relay, relay_s)
     arrived(stats.at[pl.ds(0, tp - 1)], stat_s)
     arrived(act.at[pl.ds(0, 2 * ny - 1)], act_s)
     arrived(far, dsend)
     arrived(far, bsend)
 
     def drain(i, carry):
-        arrived(rows.at[0, pl.ds(0, tp - 1)], rsend.at[i])
+        arrived(rows.at[0, 0], rsend.at[i])
+        arrived(rows.at[0, 0, pl.ds(0, ny - 1)], rsend.at[i])
         arrived(give.at[0], sib_s.at[i])
         arrived(sumout.at[0], sum_s.at[i])
         return carry
@@ -464,7 +503,7 @@
             pltpu.VMEM((tokens, 8), F32),
             pltpu.VMEM((tokens, width), BF),
             pltpu.VMEM((sp * cap, width), BF),
-            pltpu.VMEM((nz, tp, chunk, width), BF),
+            pltpu.VMEM((nz, 2, ny, chunk, width), BF),
             pltpu.VMEM((nz, ny, chunk, width), F32),
             pltpu.VMEM((nz, ny, chunk, width), BF),
             pltpu.VMEM((nz, ny, chunk, width), BF),
@@ -479,6 +518,9 @@
             dma(()),
             dma(()),
             dma((ny,)),
+            dma(()),
+            pltpu.VMEM((2, ffw, width), BF),
+            dma(()),
             dma(()),
             dma(()),
             dma(()),

time: 103 us -> 102 us (level); the launches traced: 101 us -> 102 us
  no operation moved by 1% of the time
where the time goes in v4:
time: 102 us
  Pallas kernels  100 us (98%)
  local copies, waits for them, and re-layouts  1.47 us (1%)
    pallas_call x1, Pallas kernels, per_device(): pl.pallas_call(functools.partial(layer_kernel, dims), out_shape=jax.Shape...  100 us

profile of v4, /device:TPU:1, one launch (start us, length us, event | category | flops | bytes accessed | tf_op | source)
XLA Modules:
  0.0 101.7 jit_solution(114187324193250351)
XLA Ops:
  0.0 100.2 %shard_map.118 = bf16[256,128]{1,0:T(8,128)(2,1)} custom-call(bf16[64,256]{1,0:T(8,128)(2,1)} %gv_hbm.1, bf16[64,256]{1,0:T(8,128)(2,1)} %gg_hbm.1, f32[31,64]{1,0:T(8,128)} %bitcast.5, f32[1,64]{1,0:T(1,128)} %bitcast.9, bf16[1024,128]{1,0:T(8,128)(2,1)} %proj_hbm.1, bf16[256,128]{1,0:T(8,128)(2,1)} %resid_hbm.1, s32[2,256]{1,0:T(2,128)} %bitcast.6, ...), custom_call_target="tpu_custom_call" | custom-call | tf_op jit(solution)/shard_map/pallas_call | solution.py:481
  100.2 1.5 %copy.14 = bf16[256,128]{1,0:T(8,128)(2,1)} copy(bf16[256,128]{1,0:T(8,128)(2,1)} %shard_map.118) | data formatting | bytes 131072

commit v5 on v4

--- a/solution.py
+++ b/solution.py
@@ -128,9 +128,6 @@
             )
         )
     ]
-    for load in loads:
-        load.start()
-
     barrier = pltpu.get_barrier_semaphore()
 
     for k in sorted(range(1, experts), key=lambda k: -min(k // nx, nz - k // nx)):
@@ -140,6 +137,9 @@
     for k in far_first:
         peer = (s, lax.rem(j + k, tp))
         pl.semaphore_signal(barrier, inc=1, device_id=peer, device_id_type=MESH)
+
+    for load in loads:
+        load.start()
 
     loads[0].wait()
     loads[1].wait()
@@ -178,6 +178,16 @@
     tapcol[taps : taps + 1, 0:own_ch] = gain_ref[...]
     tap = tapcol[...].T
 
+    def convolve(block):
+        total = jnp.zeros((own_ch, block.shape[1] - LANES), F32)
+        for o in range(taps):
+            shift = taps - 1 - o
+            moved = pltpu.roll(block, shift, 1) if shift else block
+            total = total + tap[0:own_ch, o : o + 1] * moved[:, LANES:]
+        return total
+
+    later = convolve(gated.astype(F32))
+
     loads[2].wait()
     wdt[j] = wd[rows_of(j, ffw), :]
 
@@ -222,12 +232,8 @@
     def _():
         arrived(halo, halo_r)
 
-    padded = jnp.concatenate([halo[...], gated], axis=1).astype(F32)
-    filtered = jnp.zeros((own_ch, tokens), F32)
-    for o in range(taps):
-        shift = taps - 1 - o
-        moved = pltpu.roll(padded, shift, 1) if shift else padded
-        filtered = filtered + tap[0:own_ch, o : o + 1] * moved[:, LANES:]
+    early = convolve(jnp.concatenate([halo[...], gated[:, :LANES]], axis=1).astype(F32))
+    filtered = jnp.concatenate([early, later], axis=1)
     stats[j, 0:1, :] = jnp.sum(filtered, axis=0, keepdims=True)
     stats[j, 1:2, :] = jnp.sum(filtered * filtered, axis=0, keepdims=True)
 

time: 102 us -> 102 us (level)
  no operation moved by 1% of the time
where the time goes in v5:
time: 102 us; the launch traced here: 101 us
  Pallas kernels  99.6 us (98%)
  local copies, waits for them, and re-layouts  1.47 us (1%)
    pallas_call x1, Pallas kernels, per_device(): pl.pallas_call(functools.partial(layer_kernel, dims), out_shape=jax.Shape...  99.6 us

profile of v5, /device:TPU:1, one launch (start us, length us, event | category | flops | bytes accessed | tf_op | source)
XLA Modules:
  0.0 101.1 jit_solution(11853754323225469012)
XLA Ops:
  0.0 99.6 %shard_map.118 = bf16[256,128]{1,0:T(8,128)(2,1)} custom-call(bf16[64,256]{1,0:T(8,128)(2,1)} %gv_hbm.1, bf16[64,256]{1,0:T(8,128)(2,1)} %gg_hbm.1, f32[31,64]{1,0:T(8,128)} %bitcast.5, f32[1,64]{1,0:T(1,128)} %bitcast.9, bf16[1024,128]{1,0:T(8,128)(2,1)} %proj_hbm.1, bf16[256,128]{1,0:T(8,128)(2,1)} %resid_hbm.1, s32[2,256]{1,0:T(2,128)} %bitcast.6, ...), custom_call_target="tpu_custom_call" | custom-call | tf_op jit(solution)/shard_map/pallas_call | solution.py:487
  99.6 1.5 %copy.14 = bf16[256,128]{1,0:T(8,128)(2,1)} copy(bf16[256,128]{1,0:T(8,128)(2,1)} %shard_map.118) | data formatting | bytes 131072
